TPU v7x, 32 devices: a whole 2x2x4 slice. The times are simulated.
32 devices in a mesh: fs: 8 (over z, x), tp: 4 (over y, core).
Axes of the slice: x: 2, y: 2, z: 4, core: 2. Of those that a mesh axis runs over, the one named last changes fastest.
Arguments:
- seq_rows: bfloat16 [6144, 2048], P('fs', 'tp'), may hold values from -6 to 6
- mixer_gain: bfloat16 [2048], P('tp'), may hold values from 0.099609375 to 1.8984375
- query_weight: bfloat16 [2048, 2048], P('fs', 'tp'), may hold values from -0.125 to 0.125
- key_weight: bfloat16 [2048, 2048], P('fs', 'tp'), may hold values from -0.125 to 0.125
- value_weight: bfloat16 [2048, 4096], P('fs', 'tp'), may hold values from -0.125 to 0.125
- decay_logs: float32 [8], P('tp'), may hold values from -0.0333333333 to -0.000390625
- mixer_out_weight: bfloat16 [4096, 2048], P('tp', 'fs'), may hold values from -0.125 to 0.125
- channel_gain: bfloat16 [2048], P('tp'), may hold values from 0.099609375 to 1.8984375
- value_up_weight: bfloat16 [2048, 5632], P('fs', 'tp'), may hold values from -0.125 to 0.125
- gate_up_weight: bfloat16 [2048, 5632], P('fs', 'tp'), may hold values from -0.125 to 0.125
- conv_taps: bfloat16 [3, 5632], P(None, 'tp'), may hold values from -3 to 3
- conv_bias: bfloat16 [5632], P('tp'), may hold values from -3 to 3
- down_weight: bfloat16 [5632, 2048], P('tp', 'fs'), may hold values from -0.109375 to 0.109375
Outputs:
- layer_out: bfloat16 [6144, 2048], P('fs', 'tp')
All inputs are finite; a program needn't handle non-finite values.
Results may differ from a plain program's by a relative error of at most 0.02.
Values may be sent and summed in bfloat16 or wider, within the bound.
A program may use at most 128 MiB of HBM per device.

v0:
```python
import jax
import jax.numpy as jnp
from jax import lax
from jax.sharding import PartitionSpec as P

DK = 256
DV = 512
KW = 3
BLOCK = 128
EPS = 1e-06
ROPE_BASE = 10000.0
HIGH_PRECISION = lax.Precision.HIGHEST


def rotate_heads(tensor, cosine, sine):
    half = tensor.shape[-1] // 2
    first = tensor[..., :half]
    second = tensor[..., half:]
    return jnp.concatenate(
        [first * cosine - second * sine, first * sine + second * cosine], axis=-1
    )


def retention_blocks(query, key, value, decay_logs):
    length, heads = (query.shape[0], query.shape[1])
    count = length // BLOCK
    offsets = jnp.arange(BLOCK, dtype=jnp.float32)
    spread = offsets[:, None] - offsets[None, :]
    within_block = jnp.where(
        spread[None] >= 0.0,
        jnp.exp(decay_logs[:, None, None] * jnp.maximum(spread, 0.0)[None]),
        0.0,
    )
    carried = jnp.exp(decay_logs[:, None] * (offsets + 1.0))
    state_decay_factor = jnp.exp(decay_logs[:, None] * (BLOCK - 1.0 - offsets))
    block_decay_factor = jnp.exp(decay_logs * BLOCK)

    def blocks(tensor):
        return tensor.reshape(count, BLOCK, heads, tensor.shape[-1]).transpose(0, 2, 1, 3)

    def advance(recurrent_state, triple):
        query_block, key_block, value_block = triple
        attention_scores = (
            jnp.einsum("ucf,uxf->ucx", query_block, key_block, precision=HIGH_PRECISION)
            * within_block
        )
        result = jnp.einsum("hnm,hmv->hnv", attention_scores, value_block, precision=HIGH_PRECISION)
        result = (
            result
            + jnp.einsum("hnd,hdv->hnv", query_block, recurrent_state, precision=HIGH_PRECISION)
            * carried[:, :, None]
        )
        recurrent_state = block_decay_factor[:, None, None] * recurrent_state + jnp.einsum(
            "ieb,iez->ibz",
            key_block * state_decay_factor[:, :, None],
            value_block,
            precision=HIGH_PRECISION,
        )
        return (recurrent_state, result)

    start = jnp.zeros((heads, query.shape[-1], value.shape[-1]), jnp.float32)
    _, result = lax.scan(advance, start, (blocks(query), blocks(key), blocks(value)))
    return result.transpose(0, 2, 1, 3).reshape(length, heads, value.shape[-1])


def normalise(whole_rows, gain_row):
    rows_f = whole_rows.astype(jnp.float32)
    factor = lax.rsqrt(jnp.mean(rows_f * rows_f, axis=-1, keepdims=True) + EPS)
    scaled = (rows_f * gain_row.astype(jnp.float32)[None, :]).astype(jnp.bfloat16)
    return (factor, scaled)


def on_device(
    seq_rows,
    mixer_gain,
    query_weight,
    key_weight,
    value_weight,
    decay_logs,
    mixer_out_weight,
    channel_gain,
    value_up_weight,
    gate_up_weight,
    conv_taps,
    conv_bias,
    down_weight,
):
    length = seq_rows.shape[0]
    hidden_part = value_up_weight.shape[1]
    heads_here = query_weight.shape[1] // DK
    whole_rows, gains = (
        lax.all_gather(seq_rows, "tp", axis=1, tiled=True),
        lax.all_gather(jnp.stack([mixer_gain, channel_gain]), "tp", axis=1, tiled=True),
    )
    factor_one, scaled_one = normalise(whole_rows, gains[0])
    pieces = (
        lax.all_gather(query_weight, "fs", axis=0, tiled=True),
        lax.all_gather(key_weight, "fs", axis=0, tiled=True),
        lax.all_gather(value_weight, "fs", axis=0, tiled=True),
    )
    columns = scaled_one
    sum_q, sum_k, sum_v = tuple(
        (jnp.dot(columns, piece, preferred_element_type=jnp.float32) for piece in pieces)
    )
    query = (sum_q * factor_one).astype(jnp.bfloat16)
    key = (sum_k * factor_one).astype(jnp.bfloat16)
    value = (sum_v * factor_one).astype(jnp.bfloat16)
    half = DK // 2
    freqs = jnp.power(ROPE_BASE, -jnp.arange(half, dtype=jnp.float32) * 2.0 / DK)
    angles = jnp.arange(length, dtype=jnp.float32)[:, None] * freqs[None, :]
    cosine = jnp.cos(angles)[:, None, :]
    sine = jnp.sin(angles)[:, None, :]
    turned_q = rotate_heads(query.astype(jnp.float32).reshape(length, heads_here, DK), cosine, sine)
    turned_k = rotate_heads(
        key.astype(jnp.float32).reshape(length, heads_here, DK), cosine, sine
    ) * DK ** (-0.5)
    ret = retention_blocks(
        turned_q, turned_k, value.astype(jnp.float32).reshape(length, heads_here, DV), decay_logs
    )
    centred = ret - jnp.mean(ret, axis=-1, keepdims=True)
    normed = (
        (centred * lax.rsqrt(jnp.mean(centred * centred, axis=-1, keepdims=True) + EPS))
        .reshape(length, heads_here * DV)
        .astype(jnp.bfloat16)
    )
    mixed_terms = jnp.dot(
        normed,
        lax.all_gather(mixer_out_weight, "fs", axis=1, tiled=True),
        preferred_element_type=jnp.float32,
    )
    mixed = lax.psum_scatter(
        mixed_terms.astype(jnp.bfloat16), "tp", scatter_dimension=1, tiled=True
    ).astype(jnp.float32)
    middle = (seq_rows.astype(jnp.float32) + mixed).astype(jnp.bfloat16)
    middle_whole = lax.all_gather(middle, "tp", axis=1, tiled=True)
    factor_two, scaled_two = normalise(middle_whole, gains[1])
    pieces = (
        lax.all_gather(value_up_weight, "fs", axis=0, tiled=True),
        lax.all_gather(gate_up_weight, "fs", axis=0, tiled=True),
    )
    columns = scaled_two
    sum_val = jnp.dot(columns, pieces[0], preferred_element_type=jnp.float32)
    sum_gate = jnp.dot(columns, pieces[1], preferred_element_type=jnp.float32)
    up_val = (sum_val * factor_two).astype(jnp.bfloat16)
    up_gate = (sum_gate * factor_two).astype(jnp.bfloat16)
    padded = jnp.concatenate(
        [jnp.zeros((KW - 1, hidden_part), jnp.float32), up_gate.astype(jnp.float32)], axis=0
    )
    conv = jnp.zeros((length, hidden_part), jnp.float32) + conv_bias.astype(jnp.float32)[None, :]
    for tap in range(KW):
        conv = conv + conv_taps[tap].astype(jnp.float32)[None, :] * padded[tap : tap + length]
    hidden = (jax.nn.silu(conv) * up_val.astype(jnp.float32)).astype(jnp.bfloat16)
    channel_terms = jnp.dot(
        hidden,
        lax.all_gather(down_weight, "fs", axis=1, tiled=True),
        preferred_element_type=jnp.float32,
    )
    channel = lax.psum_scatter(
        channel_terms.astype(jnp.bfloat16), "tp", scatter_dimension=1, tiled=True
    ).astype(jnp.float32)
    return (middle.astype(jnp.float32) + channel).astype(jnp.bfloat16)


def solution(mesh):
    placed = (
        P("fs", "tp"),
        P("tp"),
        P("fs", "tp"),
        P("fs", "tp"),
        P("fs", "tp"),
        P("tp"),
        P("tp", "fs"),
        P("tp"),
        P("fs", "tp"),
        P("fs", "tp"),
        P(None, "tp"),
        P("tp"),
        P("tp", "fs"),
    )
    return jax.shard_map(
        on_device, mesh=mesh, in_specs=placed, out_specs=P("fs", "tp"), check_vma=False
    )
```

profile of v0, /device:TPU:0, one launch (start us, length us, event | category | flops | bytes accessed | tf_op | source)
XLA Modules:
  0.0 714.1 jit_solution(16851320233970541097)
XLA Ops:
  6.5 0.7 all-gather.10.cloned.1.call-update
  7.3 0.7 all-gather.12.cloned.1.call-update
  11.5 6.2 all_gather.31
  18.3 2.2 fusion.56
  20.5 19.6 %all-gather.10.cloned.1.call-done = bf16[768,2048]{1,0:T(8,128)(2,1)} async-done(((bf16[768,512]{1,0:T(8,128)(2,1)}), bf16[768,2048]{1,0:T(8,128)(2,1)}) %all-gather.10.cloned.1.call-update) | async-done | bytes 3145744 | tf_op jit(solution)/shard_map/all_gather | solution.py:92
  40.2 2.6 fusion.31
  42.7 48.7 %all-gather.12.cloned.1.call-done = bf16[2048,512]{1,0:T(8,128)(2,1)} async-done(((bf16[256,512]{1,0:T(8,128)(2,1)}), bf16[2048,512]{1,0:T(8,128)(2,1)}) %all-gather.12.cloned.1.call-update) | async-done | bytes 2097168 | tf_op jit(solution)/shard_map/all_gather | solution.py:98
  91.4 4.4 multiply_convert_fusion.7
  96.5 44.7 %all-gather.16.cloned.1.call-done = bf16[2048,512]{1,0:T(8,128)(2,1)} async-done(((bf16[256,512]{1,0:T(8,128)(2,1)}), bf16[2048,512]{1,0:T(8,128)(2,1)}) %all-gather.16.cloned.1.call-update) | async-done | bytes 2097168 | tf_op jit(solution)/shard_map/all_gather | solution.py:97
  141.2 4.4 multiply_convert_fusion.6
  145.6 1.3 fusion.62
  146.9 1.4 copy.42
  148.3 2.3 copy.43
  150.6 1.7 multiply_subtract_fusion
  152.4 1.3 fusion.48
  153.7 60.8 %all-gather.14.cloned.1.call-done = bf16[2048,1024]{1,0:T(8,128)(2,1)} async-done(((bf16[256,1024]{1,0:T(8,128)(2,1)}), bf16[2048,1024]{1,0:T(8,128)(2,1)}) %all-gather.14.cloned.1.call-update) | async-done | bytes 4194320 | tf_op jit(solution)/shard_map/all_gather | solution.py:99
  214.5 8.2 %fusion.45 = f32[768,1024]{1,0:T(8,128)} fusion(bf16[2048,1024]{1,0:T(8,128)(2,1)} %all-gather.14.cloned.1.call-done, bf16[768,2048]{1,0:T(8,128)(2,1)} %all-gather.10.cloned.1.call-done, f32[2048]{0:T(1024)S(1)} %bitcast.94, f32[768]{0:T(1024)S(1)} %add_rsqrt_fusion.1), kind=kOutput, calls=%fused_computation.54 | convolution fusion | flops 3228303360 | bytes 10497024 | tf_op jit(solution)/shard_map/dot_general | solution.py:103
  222.7 5.6 reshape.163
  228.3 4.1 copy.48
  232.5 42.6 %while.15 = (s32[]{:T(128)}, f32[2,256,512]{2,1,0:T(8,128)S(1)}, f32[6,2,128,512]{3,2,1,0:T(8,128)}, f32[2]{0:T(128)S(1)}, f32[6,2,128,256]{3,2,0,1:T(8,128)}, /...) while((s32[]{:T(128)}, f32[2,256,512]{2,1,0:T(8,128)S(1)}, ...), condition=%wide.region_2.3_spmd.clone.clone.clone, body=%wide.region_1.2_spmd.clone.clone.clone.sunk | while | flops 1108771328 | bytes 7169184 | solution.py:62
  232.5 1.3 convolution_multiply_fusion.3
  233.8 1.6 fusion.88
  235.6 1.6 fusion.89
  237.2 2.5 convolution_add_fusion.2
  239.6 1.4 convolution_multiply_fusion.3
  241.0 1.6 fusion.88
  242.7 1.5 fusion.89
  244.2 2.5 convolution_add_fusion.2
  246.7 1.4 convolution_multiply_fusion.3
  248.1 1.6 fusion.88
  249.8 1.5 fusion.89
  251.3 2.5 convolution_add_fusion.2
  253.8 1.4 convolution_multiply_fusion.3
  255.2 1.6 fusion.88
  256.9 1.6 fusion.89
  258.5 2.5 convolution_add_fusion.2
  260.9 1.4 convolution_multiply_fusion.3
  262.3 1.6 fusion.88
  264.0 1.5 fusion.89
  265.6 2.5 convolution_add_fusion.2
  268.0 1.4 convolution_multiply_fusion.3
  269.4 1.6 fusion.88
  271.1 1.5 fusion.89
  272.6 2.5 convolution_add_fusion.2
  275.1 2.4 bitcast_reduce_fusion
  278.8 1.1 mul.367
  279.9 2.5 copy.46
  282.6 1.1 sub.65
  283.6 2.5 copy.45
  286.1 2.4 copy.34
  288.6 2.4 copy.44
  291.0 9.3 %convolution_convert_fusion = bf16[768,2048]{1,0:T(8,128)(2,1)} fusion(bf16[1024,2048]{1,0:T(8,128)(2,1)} %all-gather.18.cloned.1.call-done, f32[768,1024]{1,0:T(8,128)S(1)} %bitcast.83, f32[768,1024]{1,0:T(8,128)} %bitcast.85, f32[768,1024]{1,0:T(8,128)} %bitcast.84), kind=kOutput, calls=%fused_computation.44 | convolution fusion | flops 3225157632 | bytes 16777216 | tf_op jit(solution)/shard_map/dot_general | solution.py:126
  300.3 36.5 %reduce-scatter.3.cloned.1.call-done = bf16[768,512]{1,0:T(8,128)(2,1)} async-done(((bf16[768,2048]{1,0:T(8,128)(2,1)}), bf16[768,512]{1,0:T(8,128)(2,1)}) %reduce-scatter.3.cloned.1.call-update) | async-done | bytes 786448 | tf_op jit(solution)/shard_map/reduce_scatter | solution.py:131
  336.8 2.2 add_convert_fusion.1
  339.1 0.7 all-gather.22.cloned.1.call-update
  341.3 26.5 %all-gather.20.cloned.1.call-done = bf16[768,2048]{1,0:T(8,128)(2,1)} async-done(((bf16[768,512]{1,0:T(8,128)(2,1)}), bf16[768,2048]{1,0:T(8,128)(2,1)}) %all-gather.20.cloned.1.call-update) | async-done | bytes 3145744 | tf_op jit(solution)/shard_map/all_gather | solution.py:135
  367.7 2.7 fusion.33
  370.5 91.8 %all-gather.22.cloned.1.call-done = bf16[2048,1408]{1,0:T(8,128)(2,1)} async-done(((bf16[256,1408]{1,0:T(8,128)(2,1)}), bf16[2048,1408]{1,0:T(8,128)(2,1)}) %all-gather.22.cloned.1.call-update) | async-done | bytes 5767184 | tf_op jit(solution)/shard_map/all_gather | solution.py:139
  462.2 9.2 %fusion.34 = f32[768,1408]{1,0:T(8,128)} fusion(bf16[2048,1408]{1,0:T(8,128)(2,1)} %all-gather.22.cloned.1.call-done, bf16[768,2048]{1,0:T(8,128)(2,1)S(1)} %copy-done.2, f32[2048]{0:T(1024)S(1)} %bitcast.90, f32[768]{0:T(1024)S(1)} %add_rsqrt_fusion), kind=kOutput, calls=%fused_computation.45 | convolution fusion | flops 4437147648 | bytes 13249536 | tf_op jit(solution)/shard_map/dot_general | solution.py:143
  471.5 83.5 %all-gather.24.cloned.1.call-done = bf16[2048,1408]{1,0:T(8,128)(2,1)} async-done(((bf16[256,1408]{1,0:T(8,128)(2,1)}), bf16[2048,1408]{1,0:T(8,128)(2,1)}) %all-gather.24.cloned.1.call-update) | async-done | bytes 5767184 | tf_op jit(solution)/shard_map/all_gather | solution.py:138
  555.0 93.2 %all-gather.26.cloned.1.call-done = bf16[1408,2048]{1,0:T(8,128)(2,1)} async-done(((bf16[1408,256]{1,0:T(8,128)(2,1)}), bf16[1408,2048]{1,0:T(8,128)(2,1)}) %all-gather.26.cloned.1.call-update) | async-done | bytes 5767184 | tf_op jit(solution)/shard_map/all_gather | solution.py:155
  648.2 21.1 %convolution_convert_fusion.1 = bf16[768,2048]{1,0:T(8,128)(2,1)} fusion(bf16[1408,2048]{1,0:T(8,128)(2,1)} %all-gather.26.cloned.1.call-done, f32[768,1408]{1,0:T(8,128)} %fusion.34, bf16[2048,1408]{1,0:T(8,128)(2,1)} %all-gather.24.cloned.1.call-done, bf16[768,2048]{1,0:T(8,128)(2,1)S(1)} %copy-done.2, f32[2048]{0:T(1024)S(1)} %bitcast.91, ...), kind=kOutput, calls=%fused_computation.46 | convolution fusion | flops 8880881664 | bytes 22184960 | tf_op jit(solution)/shard_map/dot_general | solution.py:153
  669.3 36.1 %reduce-scatter.5.cloned.1.call-done = bf16[768,512]{1,0:T(8,128)(2,1)} async-done(((bf16[768,2048]{1,0:T(8,128)(2,1)}), bf16[768,512]{1,0:T(8,128)(2,1)}) %reduce-scatter.5.cloned.1.call-update) | async-done | bytes 786448 | tf_op jit(solution)/shard_map/reduce_scatter | solution.py:158
  705.4 2.2 add_convert_fusion
  (68 shorter events, 8.3 us)
Async XLA Ops:
  6.5 14.0 %copy-start.5 = (f32[2]{0:T(128)S(1)}, f32[2]{0:T(128)}, u32[]{:S(2)}) copy-start(f32[2]{0:T(128)} %param.20) | copy-start | bytes 28
  6.5 33.6 %all-gather.10.cloned.1.call-start = ((), (), s32[]{:S(2)}) async-start(), calls=%async_computation.2 | async-start | bytes 3932160 | tf_op jit(solution)/shard_map/all_gather | solution.py:92
  7.3 84.1 %all-gather.12.cloned.1.call-start = ((), (), s32[]{:S(2)}) async-start(), calls=%async_computation.3 | async-start | bytes 2359296 | tf_op jit(solution)/shard_map/all_gather | solution.py:98
  8.0 133.2 %all-gather.16.cloned.1.call-start = ((), (), s32[]{:S(2)}) async-start(), calls=%async_computation.5 | async-start | bytes 2359296 | tf_op jit(solution)/shard_map/all_gather | solution.py:97
  8.7 205.8 %all-gather.14.cloned.1.call-start = ((), (), s32[]{:S(2)}) async-start(), calls=%async_computation.4 | async-start | bytes 4718592 | tf_op jit(solution)/shard_map/all_gather | solution.py:99
  9.3 281.7 %all-gather.18.cloned.1.call-start = ((), (), s32[]{:S(2)}) async-start(), calls=%async_computation.6 | async-start | bytes 4718592 | tf_op jit(solution)/shard_map/all_gather | solution.py:128
  9.9 326.9 %reduce-scatter.3.cloned.1.call-start = ((), (), s32[]{:S(2)}) async-start(), calls=%async_computation.7 | async-start | bytes 3932160 | tf_op jit(solution)/shard_map/reduce_scatter | solution.py:131
  275.1 2.9 copy-start
  288.5 2.4 copy-start.3
  300.2 36.6 %copy-start.4 = (bf16[768,512]{1,0:T(8,128)(2,1)S(1)}, bf16[768,512]{1,0:T(8,128)(2,1)}, u32[]{:S(2)}) copy-start(bf16[768,512]{1,0:T(8,128)(2,1)} %param.15) | copy-start | bytes 2359300
  300.3 40.9 %copy-start.8 = (bf16[1408]{0:T(1024)(128)(2,1)S(1)}, bf16[1408]{0:T(1024)(128)(2,1)}, u32[]{:S(2)}) copy-start(bf16[1408]{0:T(1024)(128)(2,1)} %param.26) | copy-start | bytes 8452
  300.3 40.9 %copy-start.6 = (bf16[3,1408]{1,0:T(4,128)(2,1)S(1)}, bf16[3,1408]{1,0:T(4,128)(2,1)}, u32[]{:S(2)}) copy-start(bf16[3,1408]{1,0:T(4,128)(2,1)} %param.25) | copy-start | bytes 25348
  300.3 67.4 %all-gather.20.cloned.1.call-start = ((), (), s32[]{:S(2)}) async-start(), calls=%async_computation.8 | async-start | bytes 3932160 | tf_op jit(solution)/shard_map/all_gather | solution.py:135
  339.0 123.2 %copy-start.7 = (f32[1,2048]{1,0:T(1,128)S(1)}, f32[1,2048]{1,0:T(1,128)}, u32[]{:S(2)}) copy-start(f32[1,2048]{1,0:T(1,128)} %get-tuple-element.238) | copy-start | bytes 24580
  339.0 123.2 %all-gather.22.cloned.1.call-start = ((), (), s32[]{:S(2)}) async-start(), calls=%async_computation.9 | async-start | bytes 6488064 | tf_op jit(solution)/shard_map/all_gather | solution.py:139
  339.8 215.2 %all-gather.24.cloned.1.call-start = ((), (), s32[]{:S(2)}) async-start(), calls=%async_computation.10 | async-start | bytes 6488064 | tf_op jit(solution)/shard_map/all_gather | solution.py:138
  340.5 307.7 %all-gather.26.cloned.1.call-start = ((), (), s32[]{:S(2)}) async-start(), calls=%async_computation.11 | async-start | bytes 6488064 | tf_op jit(solution)/shard_map/all_gather | solution.py:155
  341.1 364.3 %reduce-scatter.5.cloned.1.call-start = ((), (), s32[]{:S(2)}) async-start(), calls=%async_computation.12 | async-start | bytes 3932160 | tf_op jit(solution)/shard_map/reduce_scatter | solution.py:158
  367.7 94.5 %copy-start.2 = (bf16[768,2048]{1,0:T(8,128)(2,1)S(1)}, bf16[768,2048]{1,0:T(8,128)(2,1)}, u32[]{:S(2)}) copy-start(bf16[768,2048]{1,0:T(8,128)(2,1)} %all-gather.20.cloned.1.call-done) | copy-start | bytes 9437188
  669.3 36.1 %copy-start.1 = (bf16[768,512]{1,0:T(8,128)(2,1)S(1)}, bf16[768,512]{1,0:T(8,128)(2,1)}, u32[]{:S(2)}) copy-start(bf16[768,512]{1,0:T(8,128)(2,1)} %add_convert_fusion.1) | copy-start | bytes 2359300
Sparse Core Ops, SparseCore 0:
  8.9 31.2 all-gather.9
  42.3 49.0 all-gather.11
  93.5 47.6 all-gather.15
  143.2 71.3 all-gather.13
  216.4 73.1 all-gather.17
  300.4 36.3 reduce-scatter.2
  339.2 28.5 all-gather.19
  369.9 92.2 all-gather.21
  464.4 90.4 all-gather.23
  556.8 91.2 all-gather.25
  669.4 35.9 reduce-scatter.4
where the time goes:
time: 715 us; the launch traced here: 714 us
  waiting for transfers between devices  546 us (76%)
  matrix products  98.5 us (14%)
  local copies, waits for them, and re-layouts  29.7 us (4%)
  other arithmetic  19.2 us (3%)
  between operations  13.5 us (2%)
    all_gather x1, waiting for transfers between devices, on_device(): lax.all_gather(down_weight, 'fs', axis=1, tiled=True)  93.2 us
    all_gather x1, waiting for transfers between devices, on_device(): lax.all_gather(gate_up_weight, 'fs', axis=0, tiled=True)  91.8 us
    all_gather x1, waiting for transfers between devices, on_device(): lax.all_gather(value_up_weight, 'fs', axis=0, tiled=True)  83.5 us
    all_gather x1, waiting for transfers between devices, on_device(): lax.all_gather(value_weight, 'fs', axis=0, tiled=True)  60.8 us
    all_gather x1, waiting for transfers between devices, on_device(): lax.all_gather(key_weight, 'fs', axis=0, tiled=True)  48.7 us
    all_gather x1, waiting for transfers between devices, on_device(): lax.all_gather(query_weight, 'fs', axis=0, tiled=True)  44.7 us
    reduce_scatter x1, waiting for transfers between devices, on_device(): lax.psum_scatter(mixed_terms.astype(jnp.bfloat16), 'tp', scatter_dimensio...  36.5 us
    reduce_scatter x1, waiting for transfers between devices, on_device(): lax.psum_scatter(channel_terms.astype(jnp.bfloat16), 'tp', scatter_dimens...  36.1 us
  transfers between devices with their start and end apart: 11, of which 10 were waited for; matrix products, arithmetic and copies ran while one was open for 16% of the time, Pallas kernels for 0%

commit v1 on v0

--- a/solution.py
+++ b/solution.py
@@ -95,7 +95,9 @@
     factor_one, scaled_one = normalise(whole_rows, gains[0])
     pieces = (
         lax.all_gather(query_weight, "fs", axis=0, tiled=True),
-        lax.all_gather(key_weight, "fs", axis=0, tiled=True),
+        jnp.concatenate(
+            lax.all_to_all(jnp.stack([key_weight] * lax.axis_size("fs")), "fs", 0, 0), axis=0
+        ),
         lax.all_gather(value_weight, "fs", axis=0, tiled=True),
     )
     columns = scaled_one

time: 715 us -> 671 us (0.938)
  waiting for transfers between devices: 546 us -> 495 us
  starting transfers between devices: 0.39 us -> 7.63 us
    all_gather x1 -> x0, waiting for transfers between devices: 48.7 us -> none  [on_device(): lax.all_gather(key_weight, 'fs', axis=0, tiled=True)]
    all_to_all x0 -> x1, waiting for transfers between devices: none -> 32.4 us  [on_device(): lax.all_to_all(jnp.stack([key_weight] * lax.axis_size('fs')), 'fs', 0, 0)]
    all_gather x1, waiting for transfers between devices: 44.7 us -> 16.7 us  [on_device(): lax.all_gather(query_weight, 'fs', axis=0, tiled=True)]
    all_to_all x0 -> x1, starting transfers between devices: none -> 7.28 us  [on_device(): lax.all_to_all(jnp.stack([key_weight] * lax.axis_size('fs')), 'fs', 0, 0)]
  transfers between devices with their start and end apart: 11 -> 11, of which waited for: 10 -> 10; matrix products, arithmetic and copies ran while one was open for 16% -> 17% of each run, Pallas kernels for 0% -> 0%
where the time goes in v1:
time: 671 us; the launch traced here: 670 us
  waiting for transfers between devices  495 us (74%)
  matrix products  97.9 us (15%)
  local copies, waits for them, and re-layouts  30.8 us (5%)
  other arithmetic  19.3 us (3%)
  between operations  13.8 us (2%)
  starting transfers between devices  7.63 us (1%)
    all_gather x1, waiting for transfers between devices, on_device(): lax.all_gather(down_weight, 'fs', axis=1, tiled=True)  93.4 us
    all_gather x1, waiting for transfers between devices, on_device(): lax.all_gather(gate_up_weight, 'fs', axis=0, tiled=True)  91.8 us
    all_gather x1, waiting for transfers between devices, on_device(): lax.all_gather(value_up_weight, 'fs', axis=0, tiled=True)  83.5 us
    all_gather x1, waiting for transfers between devices, on_device(): lax.all_gather(value_weight, 'fs', axis=0, tiled=True)  61 us
    reduce_scatter x1, waiting for transfers between devices, on_device(): lax.psum_scatter(mixed_terms.astype(jnp.bfloat16), 'tp', scatter_dimensio...  36.5 us
    reduce_scatter x1, waiting for transfers between devices, on_device(): lax.psum_scatter(channel_terms.astype(jnp.bfloat16), 'tp', scatter_dimens...  36.1 us
    all_to_all x1, waiting for transfers between devices, on_device(): lax.all_to_all(jnp.stack([key_weight] * lax.axis_size('fs')), 'fs', 0, 0)  32.4 us
    all_gather x1, waiting for transfers between devices, on_device(): middle_whole = lax.all_gather(middle, 'tp', axis=1, tiled=True)  26.3 us
  transfers between devices with their start and end apart: 11, of which 10 were waited for; matrix products, arithmetic and copies ran while one was open for 17% of the time, Pallas kernels for 0%

profile of v1, /device:TPU:0, one launch (start us, length us, event | category | flops | bytes accessed | tf_op | source)
XLA Modules:
  0.0 669.8 jit_solution(15204010763144161698)
XLA Ops:
  6.5 0.7 all-gather.9.cloned.1.call-update
  8.8 2.5 stack.11
  11.2 7.3 %all-to-all-start = ((bf16[8,256,512]{2,1,0:T(8,128)(2,1)}), bf16[8,256,512]{2,1,0:T(8,128)(2,1)S(1)}, u32[]{:S(2)}, u32[]{:S(2)}) async-start(bf16[8,256,512]{2,1,0:T(8,128)(2,1)} %stack.11), calls=%async_computation | async-start | bytes 4194304 | tf_op jit(solution)/shard_map/all_to_all | solution.py:99
  19.2 5.3 all_gather.28
  24.7 2.3 fusion.56
  27.5 12.7 %all-gather.9.cloned.1.call-done = bf16[768,2048]{1,0:T(8,128)(2,1)} async-done(((bf16[768,512]{1,0:T(8,128)(2,1)}), bf16[768,2048]{1,0:T(8,128)(2,1)}) %all-gather.9.cloned.1.call-update) | async-done | bytes 3145744 | tf_op jit(solution)/shard_map/all_gather | solution.py:92
  40.2 2.6 fusion.31
  42.8 32.4 %all-to-all-done = bf16[8,256,512]{2,1,0:T(8,128)(2,1)S(1)} async-done(((bf16[8,256,512]{2,1,0:T(8,128)(2,1)}), bf16[8,256,512]{2,1,0:T(8,128)(2,1)S(1)}, u32[]{:S(2)}, u32[]{:S(2)}) %all-to-all-start) | async-done | bytes 2097184 | tf_op jit(solution)/shard_map/all_to_all | solution.py:99
  75.2 3.7 multiply_convert_fusion.7
  79.6 16.7 %all-gather.13.cloned.1.call-done = bf16[2048,512]{1,0:T(8,128)(2,1)} async-done(((bf16[256,512]{1,0:T(8,128)(2,1)}), bf16[2048,512]{1,0:T(8,128)(2,1)}) %all-gather.13.cloned.1.call-update) | async-done | bytes 2097168 | tf_op jit(solution)/shard_map/all_gather | solution.py:97
  96.3 4.4 multiply_convert_fusion.6
  100.7 1.3 fusion.62
  102.0 1.4 copy.42
  103.4 2.3 copy.43
  105.7 1.8 multiply_subtract_fusion
  107.6 1.3 fusion.48
  108.8 61.0 %all-gather.11.cloned.1.call-done = bf16[2048,1024]{1,0:T(8,128)(2,1)} async-done(((bf16[256,1024]{1,0:T(8,128)(2,1)}), bf16[2048,1024]{1,0:T(8,128)(2,1)}) %all-gather.11.cloned.1.call-update) | async-done | bytes 4194320 | tf_op jit(solution)/shard_map/all_gather | solution.py:101
  169.8 8.2 %fusion.45 = f32[768,1024]{1,0:T(8,128)} fusion(bf16[2048,1024]{1,0:T(8,128)(2,1)} %all-gather.11.cloned.1.call-done, bf16[768,2048]{1,0:T(8,128)(2,1)} %all-gather.9.cloned.1.call-done, f32[2048]{0:T(1024)S(1)} %bitcast.96, f32[768]{0:T(1024)S(1)} %add_rsqrt_fusion.1), kind=kOutput, calls=%fused_computation.54 | convolution fusion | flops 3228303360 | bytes 10497024 | tf_op jit(solution)/shard_map/dot_general | solution.py:105
  178.0 5.6 reshape.169
  183.6 4.1 copy.48
  187.7 42.7 %while.15 = (s32[]{:T(128)}, f32[2,256,512]{2,1,0:T(8,128)S(1)}, f32[6,2,128,512]{3,2,1,0:T(8,128)}, f32[2]{0:T(128)S(1)}, f32[6,2,128,256]{3,2,0,1:T(8,128)}, /...) while((s32[]{:T(128)}, f32[2,256,512]{2,1,0:T(8,128)S(1)}, ...), condition=%wide.region_2.3_spmd.clone.clone.clone, body=%wide.region_1.2_spmd.clone.clone.clone.sunk | while | flops 1108771328 | bytes 7169184 | solution.py:62
  187.7 1.3 convolution_multiply_fusion.3
  189.1 1.6 fusion.88
  190.8 1.6 fusion.89
  192.4 2.4 convolution_add_fusion.2
  194.9 1.4 convolution_multiply_fusion.3
  196.2 1.6 fusion.88
  198.0 1.5 fusion.89
  199.5 2.5 convolution_add_fusion.2
  202.0 1.4 convolution_multiply_fusion.3
  203.3 1.6 fusion.88
  205.0 1.5 fusion.89
  206.6 2.5 convolution_add_fusion.2
  209.1 1.4 convolution_multiply_fusion.3
  210.5 1.6 fusion.88
  212.2 1.6 fusion.89
  213.7 2.4 convolution_add_fusion.2
  216.2 1.4 convolution_multiply_fusion.3
  217.6 1.6 fusion.88
  219.3 1.6 fusion.89
  220.9 2.5 convolution_add_fusion.2
  223.3 1.4 convolution_multiply_fusion.3
  224.7 1.6 fusion.88
  226.4 1.5 fusion.89
  227.9 2.5 convolution_add_fusion.2
  230.4 2.4 bitcast_reduce_fusion
  234.1 1.1 mul.367
  235.2 2.5 copy.46
  237.9 1.1 sub.65
  238.9 2.5 copy.45
  241.4 2.4 copy.34
  243.8 2.4 copy.44
  246.3 9.3 %convolution_convert_fusion = bf16[768,2048]{1,0:T(8,128)(2,1)} fusion(bf16[1024,2048]{1,0:T(8,128)(2,1)} %all-gather.15.cloned.1.call-done, f32[768,1024]{1,0:T(8,128)S(1)} %bitcast.84, f32[768,1024]{1,0:T(8,128)} %bitcast.86, f32[768,1024]{1,0:T(8,128)} %bitcast.85), kind=kOutput, calls=%fused_computation.44 | convolution fusion | flops 3225157632 | bytes 16777216 | tf_op jit(solution)/shard_map/dot_general | solution.py:128
  255.6 36.5 %reduce-scatter.3.cloned.1.call-done = bf16[768,512]{1,0:T(8,128)(2,1)} async-done(((bf16[768,2048]{1,0:T(8,128)(2,1)}), bf16[768,512]{1,0:T(8,128)(2,1)}) %reduce-scatter.3.cloned.1.call-update) | async-done | bytes 786448 | tf_op jit(solution)/shard_map/reduce_scatter | solution.py:133
  292.1 2.2 add_convert_fusion.1
  296.7 26.3 %all-gather.17.cloned.1.call-done = bf16[768,2048]{1,0:T(8,128)(2,1)} async-done(((bf16[768,512]{1,0:T(8,128)(2,1)}), bf16[768,2048]{1,0:T(8,128)(2,1)}) %all-gather.17.cloned.1.call-update) | async-done | bytes 3145744 | tf_op jit(solution)/shard_map/all_gather | solution.py:137
  323.0 2.7 fusion.33
  325.7 91.8 %all-gather.19.cloned.1.call-done = bf16[2048,1408]{1,0:T(8,128)(2,1)} async-done(((bf16[256,1408]{1,0:T(8,128)(2,1)}), bf16[2048,1408]{1,0:T(8,128)(2,1)}) %all-gather.19.cloned.1.call-update) | async-done | bytes 5767184 | tf_op jit(solution)/shard_map/all_gather | solution.py:141
  417.5 9.2 %fusion.34 = f32[768,1408]{1,0:T(8,128)} fusion(bf16[2048,1408]{1,0:T(8,128)(2,1)} %all-gather.19.cloned.1.call-done, bf16[768,2048]{1,0:T(8,128)(2,1)S(1)} %copy-done.2, f32[2048]{0:T(1024)S(1)} %bitcast.92, f32[768]{0:T(1024)S(1)} %add_rsqrt_fusion), kind=kOutput, calls=%fused_computation.45 | convolution fusion | flops 4437147648 | bytes 13249536 | tf_op jit(solution)/shard_map/dot_general | solution.py:145
  426.7 83.5 %all-gather.21.cloned.1.call-done = bf16[2048,1408]{1,0:T(8,128)(2,1)} async-done(((bf16[256,1408]{1,0:T(8,128)(2,1)}), bf16[2048,1408]{1,0:T(8,128)(2,1)}) %all-gather.21.cloned.1.call-update) | async-done | bytes 5767184 | tf_op jit(solution)/shard_map/all_gather | solution.py:140
  510.2 93.4 %all-gather.23.cloned.1.call-done = bf16[1408,2048]{1,0:T(8,128)(2,1)} async-done(((bf16[1408,256]{1,0:T(8,128)(2,1)}), bf16[1408,2048]{1,0:T(8,128)(2,1)}) %all-gather.23.cloned.1.call-update) | async-done | bytes 5767184 | tf_op jit(solution)/shard_map/all_gather | solution.py:157
  603.6 21.1 %convolution_convert_fusion.1 = bf16[768,2048]{1,0:T(8,128)(2,1)} fusion(bf16[1408,2048]{1,0:T(8,128)(2,1)} %all-gather.23.cloned.1.call-done, f32[768,1408]{1,0:T(8,128)} %fusion.34, bf16[2048,1408]{1,0:T(8,128)(2,1)} %all-gather.21.cloned.1.call-done, bf16[768,2048]{1,0:T(8,128)(2,1)S(1)} %copy-done.2, f32[2048]{0:T(1024)S(1)} %bitcast.93, ...), kind=kOutput, calls=%fused_computation.46 | convolution fusion | flops 8880881664 | bytes 22184960 | tf_op jit(solution)/shard_map/dot_general | solution.py:155
  624.7 36.1 %reduce-scatter.5.cloned.1.call-done = bf16[768,512]{1,0:T(8,128)(2,1)} async-done(((bf16[768,2048]{1,0:T(8,128)(2,1)}), bf16[768,512]{1,0:T(8,128)(2,1)}) %reduce-scatter.5.cloned.1.call-update) | async-done | bytes 786448 | tf_op jit(solution)/shard_map/reduce_scatter | solution.py:160
  660.8 2.2 add_convert_fusion
  (72 shorter events, 7.9 us)
Async XLA Ops:
  6.5 33.7 %all-gather.9.cloned.1.call-start = ((), (), s32[]{:S(2)}) async-start(), calls=%async_computation.3 | async-start | bytes 3932160 | tf_op jit(solution)/shard_map/all_gather | solution.py:92
  7.3 89.0 %all-gather.13.cloned.1.call-start = ((), (), s32[]{:S(2)}) async-start(), calls=%async_computation.5 | async-start | bytes 2359296 | tf_op jit(solution)/shard_map/all_gather | solution.py:97
  8.0 161.8 %all-gather.11.cloned.1.call-start = ((), (), s32[]{:S(2)}) async-start(), calls=%async_computation.4 | async-start | bytes 4718592 | tf_op jit(solution)/shard_map/all_gather | solution.py:101
  8.7 10.4 %copy-start.9 = (bf16[512]{0:T(512)(128)(2,1)S(1)}, bf16[512]{0:T(512)(128)(2,1)}, u32[]{:S(2)}) copy-start(bf16[512]{0:T(512)(128)(2,1)} %param.16) | copy-start | bytes 3076
  8.8 10.4 %copy-start.10 = (bf16[512]{0:T(512)(128)(2,1)S(1)}, bf16[512]{0:T(512)(128)(2,1)}, u32[]{:S(2)}) copy-start(bf16[512]{0:T(512)(128)(2,1)} %param.22) | copy-start | bytes 3076
  8.8 15.9 %copy-start.5 = (f32[2]{0:T(128)S(1)}, f32[2]{0:T(128)}, u32[]{:S(2)}) copy-start(f32[2]{0:T(128)} %param.20) | copy-start | bytes 28
  11.2 63.9 %all-to-all-start = ((bf16[8,256,512]{2,1,0:T(8,128)(2,1)}), bf16[8,256,512]{2,1,0:T(8,128)(2,1)S(1)}, u32[]{:S(2)}, u32[]{:S(2)}) async-start(bf16[8,256,512]{2,1,0:T(8,128)(2,1)} %stack.11), calls=%async_computation | async-start | bytes 4194304 | tf_op jit(solution)/shard_map/all_to_all | solution.py:99
  18.5 227.7 %all-gather.15.cloned.1.call-start = ((), (), s32[]{:S(2)}) async-start(), calls=%async_computation.6 | async-start | bytes 4718592 | tf_op jit(solution)/shard_map/all_gather | solution.py:130
  19.1 273.0 %reduce-scatter.3.cloned.1.call-start = ((), (), s32[]{:S(2)}) async-start(), calls=%async_computation.7 | async-start | bytes 3932160 | tf_op jit(solution)/shard_map/reduce_scatter | solution.py:133
  230.4 2.9 copy-start
  243.8 2.4 copy-start.3
  255.5 36.6 %copy-start.4 = (bf16[768,512]{1,0:T(8,128)(2,1)S(1)}, bf16[768,512]{1,0:T(8,128)(2,1)}, u32[]{:S(2)}) copy-start(bf16[768,512]{1,0:T(8,128)(2,1)} %param.15) | copy-start | bytes 2359300
  255.6 41.1 %copy-start.8 = (bf16[1408]{0:T(1024)(128)(2,1)S(1)}, bf16[1408]{0:T(1024)(128)(2,1)}, u32[]{:S(2)}) copy-start(bf16[1408]{0:T(1024)(128)(2,1)} %param.26) | copy-start | bytes 8452
  255.6 41.1 %copy-start.6 = (bf16[3,1408]{1,0:T(4,128)(2,1)S(1)}, bf16[3,1408]{1,0:T(4,128)(2,1)}, u32[]{:S(2)}) copy-start(bf16[3,1408]{1,0:T(4,128)(2,1)} %param.25) | copy-start | bytes 25348
  255.6 67.4 %all-gather.17.cloned.1.call-start = ((), (), s32[]{:S(2)}) async-start(), calls=%async_computation.8 | async-start | bytes 3932160 | tf_op jit(solution)/shard_map/all_gather | solution.py:137
  294.3 123.2 %copy-start.7 = (f32[1,2048]{1,0:T(1,128)S(1)}, f32[1,2048]{1,0:T(1,128)}, u32[]{:S(2)}) copy-start(f32[1,2048]{1,0:T(1,128)} %get-tuple-element.238) | copy-start | bytes 24580
  294.3 123.2 %all-gather.19.cloned.1.call-start = ((), (), s32[]{:S(2)}) async-start(), calls=%async_computation.9 | async-start | bytes 6488064 | tf_op jit(solution)/shard_map/all_gather | solution.py:141
  295.1 215.1 %all-gather.21.cloned.1.call-start = ((), (), s32[]{:S(2)}) async-start(), calls=%async_computation.10 | async-start | bytes 6488064 | tf_op jit(solution)/shard_map/all_gather | solution.py:140
  295.8 307.8 %all-gather.23.cloned.1.call-start = ((), (), s32[]{:S(2)}) async-start(), calls=%async_computation.11 | async-start | bytes 6488064 | tf_op jit(solution)/shard_map/all_gather | solution.py:157
  296.6 364.2 %reduce-scatter.5.cloned.1.call-start = ((), (), s32[]{:S(2)}) async-start(), calls=%async_computation.12 | async-start | bytes 3932160 | tf_op jit(solution)/shard_map/reduce_scatter | solution.py:160
  323.0 94.5 %copy-start.2 = (bf16[768,2048]{1,0:T(8,128)(2,1)S(1)}, bf16[768,2048]{1,0:T(8,128)(2,1)}, u32[]{:S(2)}) copy-start(bf16[768,2048]{1,0:T(8,128)(2,1)} %all-gather.17.cloned.1.call-done) | copy-start | bytes 9437188
  624.7 36.1 %copy-start.1 = (bf16[768,512]{1,0:T(8,128)(2,1)S(1)}, bf16[768,512]{1,0:T(8,128)(2,1)}, u32[]{:S(2)}) copy-start(bf16[768,512]{1,0:T(8,128)(2,1)} %add_convert_fusion.1) | copy-start | bytes 2359300
Sparse Core Ops, SparseCore 0:
  8.9 31.2 all-gather.8
  42.3 53.9 all-gather.12
  98.4 71.3 all-gather.10
  171.7 73.1 all-gather.14
  255.7 36.3 reduce-scatter.2
  294.5 28.4 all-gather.16
  325.2 92.2 all-gather.18
  419.7 90.4 all-gather.20
  512.3 91.2 all-gather.22
  624.8 35.8 reduce-scatter.4
